TPU v7x, 32 devices: a whole 2x2x4 slice. The times are simulated.
32 devices in a mesh: ep: 4 (over y, x), tp: 8 (over z, core).
Axes of the slice: x: 2, y: 2, z: 4, core: 2. Of those that a mesh axis runs over, the one named last changes fastest.
Arguments:
- tokens: bfloat16 [128, 4096], P('ep'), may hold values from -6 to 6
- norm_gain: float32 [4096], replicated, may hold values from 0.1 to 1.9
- group_ids: int32 [128, 1], P('ep'), may hold values from 0 to 1; in each aligned block of 32 rows (0 to 31, 32 to 63, ...) at most 32 rows name the same one
- local_ids: int32 [128, 4], P('ep'), may hold values from 0 to 7, all different within a row
- group_gate: float32 [128], P('ep'), may hold values from 0.3 to 1
- expert_gate: float32 [128, 4], P('ep'), may hold values from 0.1 to 1
- lengths: int32 [32], P('ep'), may hold values from 1 to 4, 64 in all
- w_gate: bfloat16 [16, 1024, 4096], P('ep', 'tp'), may hold values from -0.09375 to 0.09375
- w_up: bfloat16 [16, 1024, 4096], P('ep', 'tp'), may hold values from -0.09375 to 0.09375
- w_down: bfloat16 [16, 1024, 4096], P('ep', None, 'tp'), may hold values from -0.1875 to 0.1875
Outputs:
- mixed: bfloat16 [128, 4096], P('ep', 'tp')
Inputs may be any that keep to these rules, and one draw needn't show every extreme that they name: `group_ids`: among the 32 rows of one index of ep no group is named by more than 32 rows, and some index reaches 32. `local_ids`: each row names 4 different experts of its group. `lengths`: the first that many of a sequence's 4 positions are live.
All inputs are finite; a program needn't handle non-finite values. No bound on the sum of `lengths` on one device may be relied on, other than what follows from the above.
Results may differ from a plain program's by a relative error of at most 0.0065.
Values may be sent and summed in bfloat16 or wider, within the bound.
A program may use at most 64 MiB of HBM per device.

v0:
```python
import jax
import jax.numpy as jnp
from jax import lax
from jax.sharding import PartitionSpec as P

EXP_PER_GROUP = 8
STEP_TOK = 4


def norm_rows(tokens, norm_gain):
    values = tokens.astype(jnp.float32)
    scale = lax.rsqrt(jnp.mean(values * values, axis=1, keepdims=True) + 1e-06)
    return (values * scale * norm_gain).astype(jnp.bfloat16)


def live_mask(lengths, tok_rows):
    places = jnp.arange(tok_rows, dtype=jnp.int32)
    within = places % STEP_TOK
    owner = places // STEP_TOK
    seq_ids = jnp.arange(lengths.shape[0], dtype=jnp.int32)
    hits = (owner[:, None] == seq_ids[None, :]) & (within[:, None] < lengths[None, :])
    return jnp.any(hits, axis=1).astype(jnp.float32)


def expert_hidden(rows, w_gate, w_up):
    gate_part = jnp.einsum("rd,efd->ref", rows, w_gate, preferred_element_type=jnp.float32)
    up_part = jnp.einsum("rd,efd->ref", rows, w_up, preferred_element_type=jnp.float32)
    return (jax.nn.silu(gate_part) * up_part).astype(jnp.bfloat16)


def local(
    tokens, norm_gain, group_ids, local_ids, group_gate, expert_gate, lengths, w_gate, w_up, w_down
):
    highest = lax.Precision.HIGHEST
    tok_rows = tokens.shape[0]
    exp_dev = w_gate.shape[0]
    width_part = w_down.shape[2]
    ep_size = lax.axis_size("ep")
    groups = exp_dev * ep_size // EXP_PER_GROUP
    normed = norm_rows(tokens, norm_gain)
    live = live_mask(lengths, tok_rows)
    local_cols = jnp.arange(EXP_PER_GROUP, dtype=jnp.int32)
    picks = (local_ids[:, :, None] == local_cols[None, None, :]).astype(jnp.float32)
    weights = expert_gate * (group_gate * live)[:, None]
    dense = jnp.sum(picks * weights[:, :, None], axis=1)
    group_cols = jnp.arange(groups, dtype=jnp.int32)
    member_int = (group_ids == group_cols[None, :]).astype(jnp.int32)
    member = member_int.astype(jnp.float32)
    capacity = 2 * tok_rows // groups
    counts = jnp.cumsum(member_int, axis=0)
    rank = jnp.sum((counts - 1) * member_int, axis=1)
    slot_ids = jnp.arange(capacity, dtype=jnp.int32)
    select = member.T[:, None, :] * (rank[None, None, :] == slot_ids[None, :, None]).astype(
        jnp.float32
    )
    rows_by_group = jnp.einsum(
        "gct,td->gcd", select.astype(jnp.bfloat16), normed, preferred_element_type=jnp.float32
    ).astype(jnp.bfloat16)
    gates_by_group = jnp.einsum("gct,tl->gcl", select, dense, precision=highest)
    share = EXP_PER_GROUP // exp_dev
    send_rows = jnp.repeat(rows_by_group, share, axis=0)
    send_gates = gates_by_group.reshape(groups, capacity, share, exp_dev).transpose(0, 2, 1, 3)
    send_gates = send_gates.reshape(ep_size, capacity, exp_dev)
    recv_rows = lax.all_to_all(send_rows, "ep", split_axis=0, concat_axis=0, tiled=True)
    recv_gates = lax.all_to_all(send_gates, "ep", split_axis=0, concat_axis=0, tiled=True)
    slot_rows = recv_rows.reshape(ep_size * capacity, recv_rows.shape[2])
    slot_gates = recv_gates.reshape(ep_size * capacity, exp_dev)
    hidden = expert_hidden(slot_rows, w_gate, w_up)
    total = jnp.einsum(
        "ref,efd->red",
        lax.all_gather(hidden, "tp", axis=2, tiled=True),
        w_down,
        preferred_element_type=jnp.float32,
    )
    results = jnp.einsum("re,red->rd", slot_gates, total, precision=highest)
    results = results.reshape(ep_size, capacity, width_part)
    back = lax.all_to_all(results, "ep", split_axis=0, concat_axis=0, tiled=True)
    grouped = jnp.sum(back.reshape(groups, share, capacity, width_part), axis=1)
    mixed = jnp.einsum("gct,gcd->td", select, grouped, precision=highest)
    return mixed.astype(jnp.bfloat16)


def solution(mesh):
    in_specs = (
        P("ep", None),
        P(),
        P("ep", None),
        P("ep", None),
        P("ep"),
        P("ep", None),
        P("ep"),
        P("ep", "tp", None),
        P("ep", "tp", None),
        P("ep", None, "tp"),
    )
    out_specs = P("ep", "tp")
    return jax.shard_map(local, mesh=mesh, in_specs=in_specs, out_specs=out_specs, check_vma=False)
```

profile of v0, /device:TPU:0, one launch (start us, length us, event | category | flops | bytes accessed | tf_op | source)
XLA Modules:
  0.0 81.1 jit_solution(2347612556403566781)
XLA Ops:
  6.5 0.7 fusion.25
  7.2 0.7 fusion.17
  7.9 1.1 %fusion.4 = f32[32]{0:T(128)S(1)} fusion(bf16[32,4096]{1,0:T(8,128)(2,1)} %param.10), kind=kLoop, calls=%fused_computation.10 | loop fusion | flops 393184 | bytes 262272 | tf_op jit(solution)/shard_map/reduce_sum | solution.py:12
  9.0 0.1 reduce_window_sum.11
  9.1 1.0 %select_reduce_fusion.1 = s32[32]{0:T(128)S(1)} fusion(s32[32,2]{1,0:T(8,128)S(1)} %reduce_window_sum.11, s32[32]{0:T(128)} %bitcast.46), kind=kLoop, calls=%fused_computation.27 | loop fusion | flops 224 | bytes 512 | tf_op jit(solution)/shard_map/reduce_sum | solution.py:51
  10.1 0.1 fusion.21
  10.2 1.6 %convolution_convert_fusion = bf16[2,32,4096]{2,1,0:T(8,128)(2,1)S(1)} fusion(bf16[32,4096]{1,0:T(8,128)(2,1)} %param.10, f32[4096]{0:T(1024)} %param.11, f32[32]{0:T(128)S(1)} %add_rsqrt_fusion, f32[32,32]{0,1:T(8,128)S(1)} %fusion.21, f32[2,32]{1,0:T(2,128)S(1)} %fusion.25), kind=kOutput, calls=%fused_computation | convolution fusion | flops 17567744 | bytes 807296 | tf_op jit(solution)/shard_map/gct,td->gcd/dot_general | solution.py:56
  11.7 0.1 broadcast_in_dim.2
  11.8 0.0 copy-start.4
  11.8 19.4 %all_to_all.15 = bf16[4,32,4096]{2,1,0:T(8,128)(2,1)S(1)} all-to-all(bf16[4,32,4096]{2,1,0:T(8,128)(2,1)S(1)} %bitcast.37), channel_id=1, replica_groups=mesh['ep'=4,'tp'=8] {'ep'}, dimensions={0} | all-to-all | bytes 2097152 | tf_op jit(solution)/shard_map/all_to_all | solution.py:64
  31.3 1.5 %fusion.27 = f32[128,4,128]{2,0,1:T(8,128)S(1)} fusion(bf16[128,4096,1]{1,0,2:T(8,128)(2,1)S(1)} %bitcast.38, bf16[4,128,4096]{2,1,0:T(8,128)(2,1)S(1)} %copy-done), kind=kOutput, calls=%fused_computation.51 | convolution fusion | flops 536870912 | bytes 5505024 | tf_op jit(solution)/shard_map/rd,efd->ref/dot_general | solution.py:26
  32.8 0.0 copy-start.3
  32.8 0.0 copy-start.5
  32.8 0.0 copy-start.1
  32.8 0.0 copy-start.2
  32.8 2.2 %fusion = bf16[128,4,128]{2,0,1:T(8,128)(2,1)} fusion(bf16[128,4096,1]{1,0,2:T(8,128)(2,1)S(1)} %bitcast.39, bf16[4,128,4096]{2,1,0:T(8,128)(2,1)S(1)} %copy-done.4, f32[128,4,128]{2,0,1:T(8,128)S(1)} %fusion.27), kind=kOutput, calls=%fused_computation.3 | convolution fusion | flops 537264128 | bytes 5636096 | tf_op jit(solution)/shard_map/rd,efd->ref/dot_general | solution.py:27
  35.0 0.0 all-gather.2.cloned.1.call-update
  35.1 0.1 fusion.24
  35.2 0.2 fusion.12
  35.4 0.1 pad_maximum_fusion
  35.5 0.1 reshape.102
  35.6 0.1 reshape.115
  35.7 7.0 %all_to_all.16 = f32[4,1,128]{2,1,0:T(1,128)S(1)} all-to-all(f32[4,1,128]{2,1,0:T(1,128)S(1)} %reshape.115), channel_id=1, replica_groups=mesh['ep'=4,'tp'=8] {'ep'}, dimensions={0} | all-to-all | bytes 4096 | tf_op jit(solution)/shard_map/all_to_all | solution.py:65
  42.7 0.5 broadcast.120
  43.2 0.7 reduce
  43.9 0.1 reshape.116
  44.0 0.1 copy.43
  44.1 14.7 %all-gather.2.cloned.1.call-done = bf16[128,4,1024]{2,0,1:T(8,128)(2,1)} async-done(((bf16[128,4,128]{2,0,1:T(8,128)(2,1)}), bf16[128,4,1024]{2,0,1:T(8,128)(2,1)}) %all-gather.2.cloned.1.call-update) | async-done | bytes 1048592 | tf_op jit(solution)/shard_map/all_gather | solution.py:71
  58.8 3.2 %convolution_bitcast_fusion = f32[128,4,512]{2,0,1:T(8,128)S(1)} fusion(bf16[128,4,1024]{2,0,1:T(8,128)(2,1)} %all-gather.2.cloned.1.call-done, bf16[4,1024,512]{2,1,0:T(8,128)(2,1)} %param.19), kind=kOutput, calls=%fused_computation.1 | convolution fusion | flops 536870912 | bytes 6291456 | tf_op jit(solution)/shard_map/ref,efd->red/dot_general | solution.py:69
  62.0 2.4 %fusion.2 = f32[128,1,512]{2,1,0:T(1,128)S(1)} fusion(f32[128,4,1]{1,2,0:T(1,128)S(1)} %bitcast.41, f32[128,4,512]{2,0,1:T(8,128)S(1)} %convolution_bitcast_fusion), kind=kOutput, calls=%fused_computation.6 | convolution fusion | flops 3145728 | bytes 1312768 | tf_op jit(solution)/shard_map/re,red->rd/dot_general | solution.py:75
  64.5 8.8 %all_to_all.17 = f32[4,32,512]{2,1,0:T(8,128)S(1)} all-to-all(f32[4,32,512]{2,1,0:T(8,128)S(1)} %bitcast.40), channel_id=1, replica_groups=mesh['ep'=4,'tp'=8] {'ep'}, dimensions={0} | all-to-all | bytes 524288 | tf_op jit(solution)/shard_map/all_to_all | solution.py:77
  73.3 0.9 %fusion.1 = bf16[32,512]{1,0:T(8,128)(2,1)} fusion(f32[2,32,512]{2,1,0:T(8,128)S(1)} %bitcast_reduce_fusion, f32[32,32]{0,1:T(8,128)S(1)} %fusion.21, f32[2,32]{1,0:T(2,128)S(1)} %fusion.25), kind=kOutput, calls=%fused_computation.5 | convolution fusion | flops 12601344 | bytes 168192 | tf_op jit(solution)/shard_map/gct,gcd->td/dot_general | solution.py:79
  (18 shorter events, 0.1 us)
Async XLA Ops:
  6.5 52.3 %all-gather.2.cloned.1.call-start = ((), (), s32[]{:S(2)}) async-start(), calls=%async_computation.3 | async-start | bytes 1179648 | tf_op jit(solution)/shard_map/all_gather | solution.py:71
  9.1 22.2 %copy-start = (bf16[4,128,4096]{2,1,0:T(8,128)(2,1)S(1)}, bf16[4,128,4096]{2,1,0:T(8,128)(2,1)}, u32[]{:S(2)}) copy-start(bf16[4,128,4096]{2,1,0:T(8,128)(2,1)} %param.17) | copy-start | bytes 12582916
  11.8 21.0 %copy-start.4 = (bf16[4,128,4096]{2,1,0:T(8,128)(2,1)S(1)}, bf16[4,128,4096]{2,1,0:T(8,128)(2,1)}, u32[]{:S(2)}) copy-start(bf16[4,128,4096]{2,1,0:T(8,128)(2,1)} %param.18) | copy-start | bytes 12582916
  32.8 2.3 %copy-start.3 = (s32[8]{0:T(128)S(1)}, s32[8]{0:T(128)}, u32[]{:S(2)}) copy-start(s32[8]{0:T(128)} %param.16) | copy-start | bytes 100
  32.8 2.4 %copy-start.5 = (f32[32]{0:T(128)S(1)}, f32[32]{0:T(128)}, u32[]{:S(2)}) copy-start(f32[32]{0:T(128)} %param.14) | copy-start | bytes 388
  32.8 2.4 %copy-start.1 = (f32[32,4]{0,1:T(4,128)S(1)}, f32[32,4]{0,1:T(4,128)}, u32[]{:S(2)}) copy-start(f32[32,4]{0,1:T(4,128)} %param.15) | copy-start | bytes 1540
  32.8 2.4 %copy-start.2 = (s32[32,4]{0,1:T(4,128)S(1)}, s32[32,4]{0,1:T(4,128)}, u32[]{:S(2)}) copy-start(s32[32,4]{0,1:T(4,128)} %param.13) | copy-start | bytes 1540
Sparse Core Ops, SparseCore 0:
  35.2 23.5 all-gather.1
where the time goes:
time: 81.4 us; the launch traced here: 81.1 us
  blocking collectives  35.2 us (43%)
  waiting for transfers between devices  14.7 us (18%)
  between operations  13.6 us (17%)
  matrix products  12.1 us (15%)
  other arithmetic  4.48 us (6%)
  local copies, waits for them, and re-layouts  1.06 us (1%)
    all_to_all x1, blocking collectives, local(): lax.all_to_all(send_rows, 'ep', split_axis=0, concat_axis=0, tiled=True)  19.4 us
    all_gather x1, waiting for transfers between devices, local(): lax.all_gather(hidden, 'tp', axis=2, tiled=True)  14.7 us
    all_to_all x1, blocking collectives, local(): lax.all_to_all(results, 'ep', split_axis=0, concat_axis=0, tiled=True)  8.79 us
    all_to_all x1, blocking collectives, local(): lax.all_to_all(send_gates, 'ep', split_axis=0, concat_axis=0, tiled=True)  7.01 us
    dot_general x1, matrix products, local(): jnp.einsum('ref,efd->red', lax.all_gather(hidden, 'tp', axis=2, tiled=Tru...  3.23 us
    dot_general x1, matrix products, local(): results = jnp.einsum('re,red->rd', slot_gates, total, precision=highest)  2.43 us
    dot_general x1, matrix products, expert_hidden(): jnp.einsum('rd,efd->ref', rows, w_up, preferred_element_type=jnp.float32)  2.18 us
  transfers between devices with their start and end apart: 1, of which 1 were waited for; matrix products, arithmetic and copies ran while one was open for 2% of the time, Pallas kernels for 0%

commit v1 on v0

--- a/solution.py
+++ b/solution.py
@@ -66,11 +66,9 @@
     slot_rows = recv_rows.reshape(ep_size * capacity, recv_rows.shape[2])
     slot_gates = recv_gates.reshape(ep_size * capacity, exp_dev)
     hidden = expert_hidden(slot_rows, w_gate, w_up)
+    begin_samples = lambda across, message: jnp.concatenate(lax.all_gather(message, across), axis=2)
     total = jnp.einsum(
-        "ref,efd->red",
-        lax.all_gather(hidden, "tp", axis=2, tiled=True),
-        w_down,
-        preferred_element_type=jnp.float32,
+        "ref,efd->red", begin_samples("tp", hidden), w_down, preferred_element_type=jnp.float32
     )
     results = jnp.einsum("re,red->rd", slot_gates, total, precision=highest)
     results = results.reshape(ep_size, capacity, width_part)

time: 81.4 us -> 81.9 us (level)
  local copies, waits for them, and re-layouts: 1.06 us -> 2.67 us
  waiting for transfers between devices: 14.7 us -> 13.1 us
    all_gather x1, waiting for transfers between devices: 14.7 us -> 13.1 us  [local(): lax.all_gather(message, across)]
    all_gather x0 -> x1, local copies, waits for them, and re-layouts: none -> 1.61 us  [local(): lax.all_gather(message, across)]
where the time goes in v1:
time: 81.9 us; the launch traced here: 81.6 us
  blocking collectives  36 us (44%)
  between operations  13.6 us (17%)
  waiting for transfers between devices  13.1 us (16%)
  matrix products  11.8 us (14%)
  other arithmetic  4.48 us (5%)
  local copies, waits for them, and re-layouts  2.67 us (3%)
    all_to_all x1, blocking collectives, local(): lax.all_to_all(send_rows, 'ep', split_axis=0, concat_axis=0, tiled=True)  19.4 us
    all_gather x1, waiting for transfers between devices, local(): lax.all_gather(message, across)  13.1 us
    all_to_all x1, blocking collectives, local(): lax.all_to_all(results, 'ep', split_axis=0, concat_axis=0, tiled=True)  9.58 us
    all_to_all x1, blocking collectives, local(): lax.all_to_all(send_gates, 'ep', split_axis=0, concat_axis=0, tiled=True)  7.01 us
    dot_general x1, matrix products, local(): jnp.einsum('ref,efd->red', begin_samples('tp', hidden), w_down, preferred...  2.99 us
    dot_general x1, matrix products, local(): results = jnp.einsum('re,red->rd', slot_gates, total, precision=highest)  2.42 us
    dot_general x1, matrix products, expert_hidden(): jnp.einsum('rd,efd->ref', rows, w_up, preferred_element_type=jnp.float32)  2.18 us
  transfers between devices with their start and end apart: 1, of which 1 were waited for; matrix products, arithmetic and copies ran while one was open for 2% of the time, Pallas kernels for 0%

profile of v1, /device:TPU:0, one launch (start us, length us, event | category | flops | bytes accessed | tf_op | source)
XLA Modules:
  0.0 81.6 jit_solution(1017924528406726188)
XLA Ops:
  6.5 0.7 fusion.25
  7.2 0.7 fusion.17
  7.9 1.1 %fusion.4 = f32[32]{0:T(128)S(1)} fusion(bf16[32,4096]{1,0:T(8,128)(2,1)} %param.10), kind=kLoop, calls=%fused_computation.10 | loop fusion | flops 393184 | bytes 262272 | tf_op jit(solution)/shard_map/reduce_sum | solution.py:12
  9.0 0.1 reduce_window_sum.11
  9.1 1.0 %select_reduce_fusion.1 = s32[32]{0:T(128)S(1)} fusion(s32[32,2]{1,0:T(8,128)S(1)} %reduce_window_sum.11, s32[32]{0:T(128)} %bitcast.52), kind=kLoop, calls=%fused_computation.27 | loop fusion | flops 224 | bytes 512 | tf_op jit(solution)/shard_map/reduce_sum | solution.py:51
  10.1 0.1 fusion.21
  10.2 1.6 %convolution_convert_fusion = bf16[2,32,4096]{2,1,0:T(8,128)(2,1)S(1)} fusion(bf16[32,4096]{1,0:T(8,128)(2,1)} %param.10, f32[4096]{0:T(1024)} %param.11, f32[32]{0:T(128)S(1)} %add_rsqrt_fusion, f32[32,32]{0,1:T(8,128)S(1)} %fusion.21, f32[2,32]{1,0:T(2,128)S(1)} %fusion.25), kind=kOutput, calls=%fused_computation | convolution fusion | flops 17567744 | bytes 807296 | tf_op jit(solution)/shard_map/gct,td->gcd/dot_general | solution.py:56
  11.7 0.1 broadcast_in_dim.2
  11.8 0.0 copy-start.4
  11.8 19.4 %all_to_all.15 = bf16[4,32,4096]{2,1,0:T(8,128)(2,1)S(1)} all-to-all(bf16[4,32,4096]{2,1,0:T(8,128)(2,1)S(1)} %bitcast.42), channel_id=1, replica_groups=mesh['ep'=4,'tp'=8] {'ep'}, dimensions={0} | all-to-all | bytes 2097152 | tf_op jit(solution)/shard_map/all_to_all | solution.py:64
  31.3 1.5 %fusion.27 = f32[128,4,128]{2,0,1:T(8,128)S(1)} fusion(bf16[128,4096,1]{1,0,2:T(8,128)(2,1)S(1)} %bitcast.43, bf16[4,128,4096]{2,1,0:T(8,128)(2,1)S(1)} %copy-done), kind=kOutput, calls=%fused_computation.51 | convolution fusion | flops 536870912 | bytes 5505024 | tf_op jit(solution)/shard_map/rd,efd->ref/dot_general | solution.py:26
  32.8 0.0 copy-start.3
  32.8 0.0 copy-start.1
  32.8 0.0 copy-start.2
  32.8 2.2 %fusion = bf16[128,4,128]{2,0,1:T(8,128)(2,1)} fusion(bf16[128,4096,1]{1,0,2:T(8,128)(2,1)S(1)} %bitcast.44, bf16[4,128,4096]{2,1,0:T(8,128)(2,1)S(1)} %copy-done.4, f32[128,4,128]{2,0,1:T(8,128)S(1)} %fusion.27), kind=kOutput, calls=%fused_computation.3 | convolution fusion | flops 537264128 | bytes 5636096 | tf_op jit(solution)/shard_map/rd,efd->ref/dot_general | solution.py:27
  35.0 0.0 all-gather.3.cloned.1.call-update
  35.1 0.1 fusion.24
  35.2 0.2 fusion.12
  35.4 0.1 pad_maximum_fusion
  35.5 0.1 reshape.108
  35.6 0.1 reshape.124
  35.7 7.0 %all_to_all.16 = f32[4,1,128]{2,1,0:T(1,128)S(1)} all-to-all(f32[4,1,128]{2,1,0:T(1,128)S(1)} %reshape.124), channel_id=1, replica_groups=mesh['ep'=4,'tp'=8] {'ep'}, dimensions={0} | all-to-all | bytes 4096 | tf_op jit(solution)/shard_map/all_to_all | solution.py:65
  42.7 0.5 broadcast.120
  43.2 0.7 reduce
  43.9 0.1 reshape.125
  44.0 0.1 copy.51
  44.1 13.1 %all-gather.3.cloned.1.call-done = bf16[1024,4,128]{2,0,1:T(8,128)(2,1)} async-done(((bf16[128,4,128]{2,0,1:T(8,128)(2,1)}), bf16[1024,4,128]{2,0,1:T(8,128)(2,1)}) %all-gather.3.cloned.1.call-update) | async-done | bytes 1048592 | tf_op jit(solution)/shard_map/all_gather | solution.py:69
  57.2 1.6 %copy.43 = bf16[8,128,4,128]{1,3,0,2:T(8,128)(2,1)S(1)} copy(bf16[8,128,4,128]{3,1,0,2:T(8,128)(2,1)} %bitcast.45) | data formatting | bytes 2097152 | tf_op jit(solution)/shard_map/all_gather | solution.py:69
  58.8 3.0 %convolution_bitcast_fusion = f32[128,4,512]{2,0,1:T(8,128)S(1)} fusion(bf16[128,4,1024]{0,2,1:T(8,128)(2,1)S(1)} %bitcast.41, bf16[4,1024,512]{2,1,0:T(8,128)(2,1)} %param.19), kind=kOutput, calls=%fused_computation.1 | convolution fusion | flops 536870912 | bytes 6291456 | tf_op jit(solution)/shard_map/ref,efd->red/dot_general | solution.py:70
  61.8 2.4 %fusion.2 = f32[128,1,512]{2,1,0:T(1,128)S(1)} fusion(f32[128,4,1]{1,2,0:T(1,128)S(1)} %bitcast.47, f32[128,4,512]{2,0,1:T(8,128)S(1)} %convolution_bitcast_fusion), kind=kOutput, calls=%fused_computation.6 | convolution fusion | flops 3145728 | bytes 1312768 | tf_op jit(solution)/shard_map/re,red->rd/dot_general | solution.py:73
  64.2 9.6 %all_to_all.17 = f32[4,32,512]{2,1,0:T(8,128)S(1)} all-to-all(f32[4,32,512]{2,1,0:T(8,128)S(1)} %bitcast.46), channel_id=1, replica_groups=mesh['ep'=4,'tp'=8] {'ep'}, dimensions={0} | all-to-all | bytes 524288 | tf_op jit(solution)/shard_map/all_to_all | solution.py:75
  73.8 0.9 %fusion.1 = bf16[32,512]{1,0:T(8,128)(2,1)} fusion(f32[2,32,512]{2,1,0:T(8,128)S(1)} %bitcast_reduce_fusion, f32[32,32]{0,1:T(8,128)S(1)} %fusion.21, f32[2,32]{1,0:T(2,128)S(1)} %fusion.25), kind=kOutput, calls=%fused_computation.5 | convolution fusion | flops 12601344 | bytes 168192 | tf_op jit(solution)/shard_map/gct,gcd->td/dot_general | solution.py:77
  (19 shorter events, 0.1 us)
Async XLA Ops:
  6.5 50.6 %all-gather.3.cloned.1.call-start = ((), (), s32[]{:S(2)}) async-start(), calls=%async_computation.3 | async-start | bytes 1179648 | tf_op jit(solution)/shard_map/all_gather | solution.py:69
  9.1 22.2 %copy-start = (bf16[4,128,4096]{2,1,0:T(8,128)(2,1)S(1)}, bf16[4,128,4096]{2,1,0:T(8,128)(2,1)}, u32[]{:S(2)}) copy-start(bf16[4,128,4096]{2,1,0:T(8,128)(2,1)} %param.17) | copy-start | bytes 12582916
  11.8 21.0 %copy-start.4 = (bf16[4,128,4096]{2,1,0:T(8,128)(2,1)S(1)}, bf16[4,128,4096]{2,1,0:T(8,128)(2,1)}, u32[]{:S(2)}) copy-start(bf16[4,128,4096]{2,1,0:T(8,128)(2,1)} %param.18) | copy-start | bytes 12582916
  32.8 2.3 %copy-start.3 = (s32[8]{0:T(128)S(1)}, s32[8]{0:T(128)}, u32[]{:S(2)}) copy-start(s32[8]{0:T(128)} %param.16) | copy-start | bytes 100
  32.8 2.4 %copy-start.5 = (f32[32]{0:T(128)S(1)}, f32[32]{0:T(128)}, u32[]{:S(2)}) copy-start(f32[32]{0:T(128)} %param.14) | copy-start | bytes 388
  32.8 2.4 %copy-start.1 = (f32[32,4]{0,1:T(4,128)S(1)}, f32[32,4]{0,1:T(4,128)}, u32[]{:S(2)}) copy-start(f32[32,4]{0,1:T(4,128)} %param.15) | copy-start | bytes 1540
  32.8 2.4 %copy-start.2 = (s32[32,4]{0,1:T(4,128)S(1)}, s32[32,4]{0,1:T(4,128)}, u32[]{:S(2)}) copy-start(s32[32,4]{0,1:T(4,128)} %param.13) | copy-start | bytes 1540
Sparse Core Ops, SparseCore 0:
  35.2 21.9 all-gather.2
